TPU v7x, 256 devices: a 4x2x16 block of a 4x16x16 slice. The times are simulated.
256 devices in a mesh: grp: 2 (over y), fs: 16 (over z), tp: 8 (over x, core).
Axes of the slice: x: 4, y: 2, z: 16, core: 2. Of those that a mesh axis runs over, the one named last changes fastest.
The devices are a block of a 4x16x16 slice.
Arguments:
- tokens: bfloat16 [32768, 2048], P(('grp', 'fs', 'tp')), parts along dimension 0, may hold values from -6 to 6
- norm_gains: float32 [4, 2048], replicated, may hold values from 0.1 to 1.9
- query_weight: bfloat16 [2048, 2048], P('fs', 'tp'), may hold values from -0.125 to 0.125
- key_weight: bfloat16 [2048, 2048], P('fs', 'tp'), may hold values from -0.125 to 0.125
- value_weight: bfloat16 [2048, 4096], P('fs', 'tp'), may hold values from -0.125 to 0.125
- swish_weight: bfloat16 [2048, 4096], P('fs', 'tp'), may hold values from -0.125 to 0.125
- mixer_output: bfloat16 [4096, 2048], P('tp', 'fs'), may hold values from -0.09375 to 0.09375
- gate_weight: bfloat16 [2048, 3072], P('fs', 'tp'), may hold values from -0.125 to 0.125
- up_weight: bfloat16 [2048, 3072], P('fs', 'tp'), may hold values from -0.125 to 0.125
- down_weight: bfloat16 [3072, 2048], P('tp', 'fs'), may hold values from -0.109375 to 0.109375
Outputs:
- layer_output: bfloat16 [32768, 2048], P(('grp', 'fs', 'tp')), parts along dimension 0
There are 2 independent parts, one for each index of `grp`. A program takes and returns all parts, laid end to end along the dimension named above; an argument that names none is the same for every part. Nothing has to cross between parts.
All inputs are finite; a program needn't handle non-finite values.
Results may differ from a plain program's by a relative error of at most 0.02.
Values may be sent and summed in bfloat16 or wider, within the bound.
A program may use at most 64 MiB of HBM per device.

v0:
```python
import jax
import jax.numpy as jnp
from jax import lax
from jax.sharding import PartitionSpec as P

H = 8
QK = 256
BLOCK = 128
norm_epsilon = 1e-06
group_epsilon = 0.01


def laid_out(pieces, dim):
    lengths = list(pieces.shape[1:])
    lengths[dim] *= pieces.shape[0]
    return jnp.moveaxis(pieces, 0, dim).reshape(lengths)


def from_everyone(array, axis):
    copies = jnp.broadcast_to(array, (lax.axis_size(axis), *array.shape))
    return lax.all_to_all(copies, axis, split_axis=0, concat_axis=0, tiled=True)


def gather_directly(array, axis, dim):
    return laid_out(from_everyone(array, axis), dim)


def split_up(array, dim, count):
    before, after = (array.shape[:dim], array.shape[dim + 1 :])
    return jnp.moveaxis(array.reshape(*before, count, -1, *after), dim, 0)


def summed_on_arrival(array, axis, dim):
    count = lax.axis_size(axis)
    pieces = lax.all_to_all(split_up(array, dim, count), axis, 0, 0, tiled=True)
    return jnp.sum(pieces.astype(jnp.float32), axis=0)


def sent_together(arrays, axis, dim, along):
    ends, at = ([], 0)
    for a in arrays[:-1]:
        at += a.shape[along]
        ends.append(at)
    both = jnp.concatenate(arrays, axis=along)
    return tuple(jnp.split(lax.all_gather(both, axis, axis=dim, tiled=True), ends, axis=along))


def rms_scale(matrix, gain):
    return (
        matrix * lax.rsqrt(jnp.mean(matrix * matrix, axis=-1, keepdims=True) + norm_epsilon) * gain
    )


def gather_rows(normed):
    return lax.all_gather(normed, "tp", axis=0, tiled=True)


def add_piece(normed, shard_piece):
    return jnp.dot(normed, shard_piece, preferred_element_type=jnp.float32)


def project_out(active, weight_shard):
    whole_weight = gather_directly(weight_shard, "fs", 1)
    return summed_on_arrival(
        jnp.dot(active, whole_weight, preferred_element_type=jnp.float32).astype(jnp.bfloat16),
        "tp",
        0,
    )


def rotate_halves(head_tensors, cosine_table, sine_table):
    half_width = head_tensors.shape[-1] // 2
    lower_half = head_tensors[..., :half_width]
    upper_half = head_tensors[..., half_width:]
    return jnp.concatenate(
        [
            lower_half * cosine_table - upper_half * sine_table,
            lower_half * sine_table + upper_half * cosine_table,
        ],
        axis=-1,
    )


def retention(queries, key_rows, value_rows, log_decay):
    length, head_count, key_width = queries.shape
    value_width = value_rows.shape[-1]
    blocks = length // BLOCK
    query_blocks = queries.reshape(blocks, BLOCK, head_count, key_width)
    key_blocks = key_rows.reshape(blocks, BLOCK, head_count, key_width)
    value_blocks = value_rows.reshape(blocks, BLOCK, head_count, value_width)
    offsets = jnp.arange(BLOCK, dtype=jnp.float32)
    distance = offsets[:, None] - offsets[None, :]
    within = jnp.where(
        distance >= 0, jnp.exp(log_decay[:, None, None] * jnp.maximum(distance, 0.0)), 0.0
    )
    retention_scores = jnp.einsum(
        "cnhd,cmhd->chnm", query_blocks, key_blocks, preferred_element_type=jnp.float32
    )
    local_part = jnp.einsum(
        "chnm,cmhe->cnhe", retention_scores * within[None], value_blocks.astype(jnp.float32)
    )
    key_decay = jnp.exp((BLOCK - 1.0 - offsets)[:, None] * log_decay[None, :])
    query_decay = jnp.exp((offsets + 1.0)[:, None] * log_decay[None, :])
    block_decay = jnp.exp(BLOCK * log_decay)

    def advance(carry_state, inputs):
        query_block, key_block, value_tile = inputs
        carried = (
            jnp.einsum("nhd,hde->nhe", query_block.astype(jnp.float32), carry_state)
            * query_decay[:, :, None]
        )
        decay_weighted = key_block.astype(jnp.float32) * key_decay[:, :, None]
        carry_state = carry_state * block_decay[:, None, None] + jnp.einsum(
            "yui,yua->uia", decay_weighted, value_tile.astype(jnp.float32)
        )
        return (carry_state, carried)

    starting_state = jnp.zeros((head_count, key_width, value_width), jnp.float32)
    _, carried = lax.scan(advance, starting_state, (query_blocks, key_blocks, value_blocks))
    return (local_part + carried).reshape(length, head_count, value_width)


def per_device(
    tokens,
    norm_gains,
    query_weight,
    key_weight,
    value_weight,
    swish_weight,
    mixer_output,
    gate_weight,
    up_weight,
    down_weight,
):
    residual = tokens.astype(jnp.float32)
    normed = gather_rows(rms_scale(residual, norm_gains[0]).astype(jnp.bfloat16))
    gate_whole, up_whole = sent_together((gate_weight, up_weight), "fs", 0, 1)
    pieces = sent_together((query_weight, key_weight, value_weight, swish_weight), "fs", 0, 1)
    raw_query, raw_keys, raw_values, raw_swish = tuple(
        (add_piece(normed, shard_piece) for shard_piece in pieces)
    )
    length = normed.shape[0]
    head_count = raw_query.shape[1] // QK
    positions = jnp.arange(length, dtype=jnp.float32)
    frequency = 10000.0 ** (-jnp.linspace(0.0, 1.0, QK // 2, dtype=jnp.float32))
    angles = positions[:, None] * frequency[None, :]
    cosine_table = jnp.cos(angles)[:, None, :]
    sine_table = jnp.sin(angles)[:, None, :]
    queries = rotate_halves(
        raw_query.reshape(length, head_count, QK), cosine_table, sine_table
    ).astype(jnp.bfloat16)
    key_rows = (
        rotate_halves(raw_keys.reshape(length, head_count, QK), cosine_table, sine_table)
        * QK ** (-0.5)
    ).astype(jnp.bfloat16)
    value_rows = raw_values.reshape(length, head_count, -1).astype(jnp.bfloat16)
    head_index = (lax.axis_index("tp") * head_count + jnp.arange(head_count)).astype(jnp.float32)
    log_decay = -(4.0 / BLOCK) * (BLOCK / (32.0 * length)) ** (head_index / (H - 1))
    retained = retention(queries, key_rows, value_rows, log_decay)
    centred = retained - jnp.mean(retained, axis=-1, keepdims=True)
    normalized = centred * lax.rsqrt(
        jnp.mean(centred * centred, axis=-1, keepdims=True) + group_epsilon
    )
    gated_rows = (jax.nn.silu(raw_swish) * normalized.reshape(length, -1)).astype(jnp.bfloat16)
    mixer_total = project_out(gated_rows, mixer_output)
    after_mixer = residual + rms_scale(mixer_total, norm_gains[1])
    widened = gather_rows(rms_scale(after_mixer, norm_gains[2]).astype(jnp.bfloat16))
    gate_sum = jnp.dot(widened, gate_whole, preferred_element_type=jnp.float32)
    up_sum = jnp.dot(widened, up_whole, preferred_element_type=jnp.float32)
    hidden = (jax.nn.silu(gate_sum) * up_sum).astype(jnp.bfloat16)
    channel = project_out(hidden, down_weight)
    return (after_mixer + rms_scale(channel, norm_gains[3])).astype(jnp.bfloat16)


def solution(mesh):
    placed = (
        P(("grp", "fs", "tp"), None),
        P(),
        P("fs", "tp"),
        P("fs", "tp"),
        P("fs", "tp"),
        P("fs", "tp"),
        P("tp", "fs"),
        P("fs", "tp"),
        P("fs", "tp"),
        P("tp", "fs"),
    )
    return jax.shard_map(
        per_device,
        mesh=mesh,
        in_specs=placed,
        out_specs=P(("grp", "fs", "tp"), None),
        check_vma=False,
    )
```

profile of v0, /device:TPU:33, one launch (start us, length us, event | category | flops | bytes accessed | tf_op | source)
XLA Modules:
  0.0 461.9 jit_solution(14256166903097563935)
XLA Ops:
  6.6 1.0 fusion.72
  7.6 1.2 fusion.39
  8.8 2.0 fusion.41
  11.0 0.8 pad_maximum_fusion.1
  11.9 0.1 copy.23
  12.0 1.5 broadcast_in_dim.19
  13.5 24.7 %all-to-all-start = ((bf16[16,512,128]{1,2,0:T(8,128)(2,1)}), bf16[16,512,128]{1,2,0:T(8,128)(2,1)}, u32[]{:S(2)}, u32[]{:S(2)}) async-start(bf16[16,512,128]{1,2,0:T(8,128)(2,1)} %broadcast_in_dim.19), calls=%async_computation | async-start | bytes 4194304 | tf_op jit(solution)/shard_map/all_to_all | solution.py:21
  38.3 0.7 pad_maximum_fusion.2
  39.3 0.1 fusion.63
  39.4 24.8 %all-gather.5.cloned.1.call-done = bf16[1024,2048]{1,0:T(8,128)(2,1)} async-done(((bf16[128,2048]{1,0:T(8,128)(2,1)}), bf16[1024,2048]{1,0:T(8,128)(2,1)}) %all-gather.5.cloned.1.call-update) | async-done | bytes 4194320 | tf_op jit(solution)/shard_map/all_gather | solution.py:55
  64.2 130.5 %all-gather.7.cloned.1.call-done = bf16[2048,1536]{1,0:T(8,128)(2,1)} async-done(((bf16[128,1536]{1,0:T(8,128)(2,1)}), bf16[2048,1536]{1,0:T(8,128)(2,1)}) %all-gather.7.cloned.1.call-update) | async-done | bytes 6291472 | tf_op jit(solution)/shard_map/all_gather | solution.py:45
  194.7 3.9 convolution_bitcast_fusion.2
  198.6 0.5 copy-done.10
  199.1 3.4 convolution_bitcast_fusion.3
  202.5 2.3 subtract_convert_fusion
  204.8 0.9 pad_maximum_fusion
  205.7 1.1 fusion.45
  206.8 3.3 fusion.36
  210.1 25.3 %while.15 = (s32[]{:T(128)}, f32[1,256,512]{2,1,0:T(8,128)S(1)}, f32[8,128,1,512]{3,1,2,0:T(8,128)}, f32[1]{0:T(128)}, bf16[8,128,1,256]{3,2,1,0:T(2,128)(2,1)S(...) while((s32[]{:T(128)}, f32[1,256,512]{2,1,0:T(8,128)S(1)}, ...), condition=%wide.region_2.3_spmd.clone.clone.clone, body=%wide.region_1.2_spmd.clone.clone.clone.sunk | while | flops 67797504 | bytes 2232440 | solution.py:119
  210.2 1.7 fusion.99
  211.9 0.2 convert_multiply_fusion.4
  212.1 1.2 fusion.98
  213.3 1.8 fusion.99
  215.1 0.2 convert_multiply_fusion.4
  215.3 1.2 fusion.98
  216.5 1.7 fusion.99
  218.3 0.2 convert_multiply_fusion.4
  218.5 1.2 fusion.98
  219.7 1.7 fusion.99
  221.4 0.2 convert_multiply_fusion.4
  221.6 1.2 fusion.98
  222.8 1.7 fusion.99
  224.6 0.2 convert_multiply_fusion.4
  224.8 1.2 fusion.98
  226.0 1.7 fusion.99
  227.7 0.2 convert_multiply_fusion.4
  228.0 1.2 fusion.98
  229.2 1.8 fusion.99
  230.9 0.2 convert_multiply_fusion.4
  231.1 1.2 fusion.98
  232.3 1.7 fusion.99
  234.1 0.2 convert_multiply_fusion.4
  234.3 1.2 fusion.98
  235.5 2.7 fusion.73
  238.2 0.4 multiply_reduce_fusion
  238.6 5.6 %fusion.27 = bf16[1024,512]{1,0:T(8,128)(2,1)S(1)} fusion(f32[8,128,1,512]{3,1,0,2:T(8,128)S(1)} %get-tuple-element.179, bf16[1024,2048]{1,0:T(8,128)(2,1)} %all-gather.5.cloned.1.call-done, bf16[2048,1536]{1,0:T(8,128)(2,1)} %all-gather.7.cloned.1.call-done, f32[1024]{0:T(1024)S(1)} %rsqrt_bitcast_fusion, f32[1024]{0:T(1024)S(1)} %get-tuple-element.174), kind=kOutput, calls=%fused_computation.36 | convolution fusion | flops 2151677952 | bytes 9445376 | tf_op jit(solution)/shard_map/dot_general | solution.py:59
  244.2 4.0 convolution_convert_fusion.1
  248.2 56.0 %all_to_all.20 = bf16[8,128,2048]{2,1,0:T(8,128)(2,1)S(1)} all-to-all(bf16[8,128,2048]{2,1,0:T(8,128)(2,1)S(1)} %bitcast.130), channel_id=1, replica_groups=mesh['grp'=2,'fs'=16,'tp'=8] {'tp'}, dimensions={0} | all-to-all | bytes 8388608 | tf_op jit(solution)/shard_map/all_to_all | solution.py:35
  304.2 0.7 convert_reduce_fusion.1
  304.9 0.2 multiply_reduce_fusion.3
  305.1 0.2 copy-done
  305.3 0.4 multiply_reduce_fusion.2
  305.6 1.1 multiply_convert_fusion.1
  306.8 0.1 copy.24
  306.9 1.4 broadcast_in_dim.20
  308.3 8.1 %all-to-all-start.2 = ((bf16[16,384,128]{1,2,0:T(8,128)(2,1)}), bf16[16,384,128]{1,2,0:T(8,128)(2,1)S(1)}, u32[]{:S(2)}, u32[]{:S(2)}) async-start(bf16[16,384,128]{1,2,0:T(8,128)(2,1)} %broadcast_in_dim.20), calls=%async_computation.2 | async-start | bytes 3145728 | tf_op jit(solution)/shard_map/all_to_all | solution.py:21
  316.4 25.5 %all-gather.9.cloned.1.call-done = bf16[1024,2048]{1,0:T(8,128)(2,1)} async-done(((bf16[128,2048]{1,0:T(8,128)(2,1)}), bf16[1024,2048]{1,0:T(8,128)(2,1)}) %all-gather.9.cloned.1.call-update) | async-done | bytes 4194320 | tf_op jit(solution)/shard_map/all_gather | solution.py:55
  342.0 6.2 %fusion.30 = f32[1024,384]{1,0:T(8,128)} fusion(bf16[1024,2048]{1,0:T(8,128)(2,1)} %all-gather.9.cloned.1.call-done, bf16[2048,768]{1,0:T(8,128)(2,1)} %all-gather.11.cloned.1.call-done), kind=kOutput, calls=%fused_computation.40 | convolution fusion | flops 1610612736 | bytes 7340032 | tf_op jit(solution)/shard_map/dot_general | solution.py:168
  348.1 37.1 %all-to-all-done.2 = bf16[16,384,128]{1,2,0:T(8,128)(2,1)S(1)} async-done(((bf16[16,384,128]{1,2,0:T(8,128)(2,1)}), bf16[16,384,128]{1,2,0:T(8,128)(2,1)S(1)}, u32[]{:S(2)}, u32[]{:S(2)}) %all-to-all-start.2) | async-done | bytes 1572896 | tf_op jit(solution)/shard_map/all_to_all | solution.py:21
  385.3 9.6 %convolution_convert_fusion = bf16[1024,2048]{1,0:T(8,128)(2,1)} fusion(bf16[384,2048]{0,1:T(8,128)(2,1)S(1)} %bitcast.137, f32[1024,384]{1,0:T(8,128)} %fusion.30, bf16[1024,2048]{1,0:T(8,128)(2,1)} %all-gather.9.cloned.1.call-done, bf16[2048,768]{1,0:T(8,128)(2,1)} %all-gather.11.cloned.1.call-done), kind=kOutput, calls=%fused_computation.26 | convolution fusion | flops 3225681920 | bytes 13107200 | tf_op jit(solution)/shard_map/dot_general | solution.py:65
  394.9 58.4 %all_to_all.21 = bf16[8,128,2048]{2,1,0:T(8,128)(2,1)S(1)} all-to-all(bf16[8,128,2048]{2,1,0:T(8,128)(2,1)} %bitcast.129), channel_id=1, replica_groups=mesh['grp'=2,'fs'=16,'tp'=8] {'tp'}, dimensions={0} | all-to-all | bytes 8388608 | tf_op jit(solution)/shard_map/all_to_all | solution.py:35
  453.2 0.7 convert_reduce_fusion
  454.0 0.2 multiply_reduce_fusion.1
  454.1 1.2 add_convert_fusion
  (50 shorter events, 0.8 us)
Async XLA Ops:
  6.5 4.4 copy-start.9
  6.5 4.5 copy-start.8
  6.6 4.5 copy-start.4
  6.6 4.5 copy-start.3
  6.6 5.3 %copy-start.2 = (bf16[512,128]{1,0:T(8,128)(2,1)S(1)}, bf16[512,128]{1,0:T(8,128)(2,1)}, u32[]{:S(2)}) copy-start(bf16[512,128]{1,0:T(8,128)(2,1)} %param.18) | copy-start | bytes 393220
  6.6 57.6 %all-gather.5.cloned.1.call-start = ((), (), s32[]{:S(2)}) async-start(), calls=%async_computation.4 | async-start | bytes 4718592 | tf_op jit(solution)/shard_map/all_gather | solution.py:55
  10.9 183.8 %all-gather.7.cloned.1.call-start = ((), (), s32[]{:S(2)}) async-start(), calls=%async_computation.5 | async-start | bytes 6684672 | tf_op jit(solution)/shard_map/all_gather | solution.py:45
  13.5 24.7 %copy-start.6 = (bf16[128,384]{1,0:T(8,128)(2,1)S(1)}, bf16[128,384]{1,0:T(8,128)(2,1)}, u32[]{:S(2)}) copy-start(bf16[128,384]{1,0:T(8,128)(2,1)} %param.20) | copy-start | bytes 294916
  13.5 24.7 %copy-start.7 = (bf16[128,384]{1,0:T(8,128)(2,1)S(1)}, bf16[128,384]{1,0:T(8,128)(2,1)}, u32[]{:S(2)}) copy-start(bf16[128,384]{1,0:T(8,128)(2,1)} %param.19) | copy-start | bytes 294916
  13.5 230.7 %all-to-all-start = ((bf16[16,512,128]{1,2,0:T(8,128)(2,1)}), bf16[16,512,128]{1,2,0:T(8,128)(2,1)}, u32[]{:S(2)}, u32[]{:S(2)}) async-start(bf16[16,512,128]{1,2,0:T(8,128)(2,1)} %broadcast_in_dim.19), calls=%async_computation | async-start | bytes 4194304 | tf_op jit(solution)/shard_map/all_to_all | solution.py:21
  38.2 278.3 %all-gather.11.cloned.1.call-start = ((), (), s32[]{:S(2)}) async-start(), calls=%async_computation.7 | async-start | bytes 3342336 | tf_op jit(solution)/shard_map/all_gather | solution.py:45
  39.0 302.9 %all-gather.9.cloned.1.call-start = ((), (), s32[]{:S(2)}) async-start(), calls=%async_computation.6 | async-start | bytes 4718592 | tf_op jit(solution)/shard_map/all_gather | solution.py:55
  194.7 4.4 copy-start.10
  202.5 4.3 copy-start.11
  204.8 5.3 %copy-start.1 = (bf16[1024,1,128]{2,0,1:T(8,128)(2,1)}, bf16[1024,1,128]{2,0,1:T(8,128)(2,1)S(1)}, u32[]{:S(2)}) copy-start(bf16[1024,1,128]{2,0,1:T(8,128)(2,1)S(1)} %get-tuple-element.167) | copy-start | bytes 786436
  304.2 1.0 copy-start
  305.3 1.5 copy-start.5
  308.3 77.0 %all-to-all-start.2 = ((bf16[16,384,128]{1,2,0:T(8,128)(2,1)}), bf16[16,384,128]{1,2,0:T(8,128)(2,1)S(1)}, u32[]{:S(2)}, u32[]{:S(2)}) async-start(bf16[16,384,128]{1,2,0:T(8,128)(2,1)} %broadcast_in_dim.20), calls=%async_computation.2 | async-start | bytes 3145728 | tf_op jit(solution)/shard_map/all_to_all | solution.py:21
Sparse Core Ops, SparseCore 0:
  11.0 53.0 all-gather.4
  66.0 128.6 all-gather.6
  196.5 65.3 all-gather.10
  306.9 34.9 all-gather.8
where the time goes:
time: 463 us; the launch traced here: 462 us
  waiting for transfers between devices  218 us (47%)
  blocking collectives  114 us (25%)
  matrix products  62 us (13%)
  starting transfers between devices  33 us (7%)
  other arithmetic  15.7 us (3%)
  between operations  13.5 us (3%)
  local copies, waits for them, and re-layouts  4.77 us (1%)
    all_gather x2, waiting for transfers between devices, sent_together(): lax.all_gather(both, axis, axis=dim, tiled=True)  131 us
    all_to_all x2, blocking collectives, summed_on_arrival(): pieces = lax.all_to_all(split_up(array, dim, count), axis, 0, 0, tiled=True)  114 us
    all_gather x2, waiting for transfers between devices, gather_rows(): return lax.all_gather(normed, 'tp', axis=0, tiled=True)  50.3 us
    all_to_all x2, waiting for transfers between devices, from_everyone(): return lax.all_to_all(copies, axis, split_axis=0, concat_axis=0, tiled=True)  37.1 us
    all_to_all x2, starting transfers between devices, from_everyone(): return lax.all_to_all(copies, axis, split_axis=0, concat_axis=0, tiled=True)  32.7 us
    dot_general x4, matrix products, add_piece(): return jnp.dot(normed, shard_piece, preferred_element_type=jnp.float32)  16.2 us
    dot_general x8, matrix products, advance(): jnp.einsum('nhd,hde->nhe', query_block.astype(jnp.float32), carry_state)  14 us
    dot_general x2, matrix products, project_out(): jnp.dot(active, whole_weight, preferred_element_type=jnp.float32)  13.6 us
  transfers between devices with their start and end apart: 6, of which 4 were waited for; matrix products, arithmetic and copies ran while one was open for 14% of the time, Pallas kernels for 0%

commit v1 on v0

--- a/solution.py
+++ b/solution.py
@@ -8,6 +8,19 @@
 BLOCK = 128
 norm_epsilon = 1e-06
 group_epsilon = 0.01
+
+
+def collect(x, axis, dim):
+    devices, index, rows = (lax.axis_size(axis), lax.axis_index(axis), x.shape[dim])
+    forward = [(i, (i + 1) % devices) for i in range(devices)]
+    whole = jnp.zeros((*x.shape[:dim], devices * rows, *x.shape[dim + 1 :]), x.dtype)
+    carried = x
+    for step in range(devices):
+        source = (index - step) % devices
+        whole = lax.dynamic_update_slice_in_dim(whole, carried, source * rows, axis=dim)
+        if step < devices - 1:
+            carried = lax.ppermute(carried, axis, forward)
+    return whole
 
 
 def laid_out(pieces, dim):
@@ -52,7 +65,7 @@
 
 
 def gather_rows(normed):
-    return lax.all_gather(normed, "tp", axis=0, tiled=True)
+    return collect(normed, "tp", 0)
 
 
 def add_piece(normed, shard_piece):

time: 463 us -> 476 us (1.028)
  blocking collectives: 114 us -> 60.7 us
  waiting for transfers between devices: 218 us -> 247 us
  local copies, waits for them, and re-layouts: 4.77 us -> 22.6 us
  starting transfers between devices: 33 us -> 45.2 us
  matrix products: 62 us -> 67.6 us
    ppermute x0 -> x14, waiting for transfers between devices: none -> 101 us  [collect(): carried = lax.ppermute(carried, axis, forward)]
    all_to_all x2 -> x1, blocking collectives: 114 us -> 60.7 us  [summed_on_arrival(): pieces = lax.all_to_all(split_up(array, dim, count), axis, 0, 0, tiled=True)]
    all_gather x2 -> x0, waiting for transfers between devices: 50.3 us -> none  [gather_rows(): return lax.all_gather(normed, 'tp', axis=0, tiled=True)]
    all_to_all x0 -> x1, waiting for transfers between devices: none -> 47.9 us  [summed_on_arrival(): pieces = lax.all_to_all(split_up(array, dim, count), axis, 0, 0, tiled=True)]
    all_to_all x2, waiting for transfers between devices: 37.1 us -> 0.01 us  [from_everyone(): return lax.all_to_all(copies, axis, split_axis=0, concat_axis=0, tiled=True)]
    all_gather x2, waiting for transfers between devices: 131 us -> 98.2 us  [sent_together(): lax.all_gather(both, axis, axis=dim, tiled=True)]
    ppermute x0 -> x14, starting transfers between devices: none -> 19.1 us  [collect(): carried = lax.ppermute(carried, axis, forward)]
    all_to_all x2, starting transfers between devices: 32.7 us -> 17.3 us  [from_everyone(): return lax.all_to_all(copies, axis, split_axis=0, concat_axis=0, tiled=True)]
  transfers between devices with their start and end apart: 6 -> 19, of which waited for: 4 -> 15; matrix products, arithmetic and copies ran while one was open for 14% -> 19% of each run, Pallas kernels for 0% -> 0%
where the time goes in v1:
time: 476 us; the launch traced here: 475 us
  waiting for transfers between devices  247 us (52%)
  matrix products  67.6 us (14%)
  blocking collectives  60.7 us (13%)
  starting transfers between devices  45.2 us (9%)
  local copies, waits for them, and re-layouts  22.6 us (5%)
  other arithmetic  18.1 us (4%)
  between operations  13.9 us (3%)
    ppermute x14, waiting for transfers between devices, collect(): carried = lax.ppermute(carried, axis, forward)  101 us
    all_gather x2, waiting for transfers between devices, sent_together(): lax.all_gather(both, axis, axis=dim, tiled=True)  98.2 us
    all_to_all x1, blocking collectives, summed_on_arrival(): pieces = lax.all_to_all(split_up(array, dim, count), axis, 0, 0, tiled=True)  60.7 us
    all_to_all x1, waiting for transfers between devices, summed_on_arrival(): pieces = lax.all_to_all(split_up(array, dim, count), axis, 0, 0, tiled=True)  47.9 us
    dot_general x4, matrix products, add_piece(): return jnp.dot(normed, shard_piece, preferred_element_type=jnp.float32)  19.4 us
    ppermute x14, starting transfers between devices, collect(): carried = lax.ppermute(carried, axis, forward)  19.1 us
    all_to_all x2, starting transfers between devices, from_everyone(): return lax.all_to_all(copies, axis, split_axis=0, concat_axis=0, tiled=True)  17.3 us
    dot_general x2, matrix products, project_out(): jnp.dot(active, whole_weight, preferred_element_type=jnp.float32)  15.8 us
  transfers between devices with their start and end apart: 19, of which 15 were waited for; matrix products, arithmetic and copies ran while one was open for 19% of the time, Pallas kernels for 0%

profile of v1, /device:TPU:33, one launch (start us, length us, event | category | flops | bytes accessed | tf_op | source)
XLA Modules:
  0.0 475.2 jit_solution(3221522254193672966)
XLA Ops:
  6.6 1.8 pad_maximum_fusion.1
  8.5 1.2 fusion.37
  10.7 2.6 broadcast.249.clone
  14.2 2.7 collective-permute-start
  16.9 19.1 %collective-permute-done = bf16[128,2048]{1,0:T(8,128)(2,1)S(1)} collective-permute-done((bf16[128,2048]{1,0:T(8,128)(2,1)S(1)}, bf16[128,2048]{1,0:T(8,128)(2,1)S(1)}, u32[]{:S(2)}, u32[]{:S(2)}) %collective-permute-start) | collective-permute-done | bytes 524320 | tf_op jit(solution)/shard_map/ppermute | solution.py:22
  36.0 9.8 %collective-permute-done.1 = bf16[128,2048]{1,0:T(8,128)(2,1)S(1)} collective-permute-done((bf16[128,2048]{1,0:T(8,128)(2,1)S(1)}, bf16[128,2048]{1,0:T(8,128)(2,1)S(1)}, u32[]{:S(2)}, u32[]{:S(2)}) %collective-permute-start.1) | collective-permute-done | bytes 524320 | tf_op jit(solution)/shard_map/ppermute | solution.py:22
  45.9 9.8 %collective-permute-done.2 = bf16[128,2048]{1,0:T(8,128)(2,1)S(1)} collective-permute-done((bf16[128,2048]{1,0:T(8,128)(2,1)S(1)}, bf16[128,2048]{1,0:T(8,128)(2,1)S(1)}, u32[]{:S(2)}, u32[]{:S(2)}) %collective-permute-start.2) | collective-permute-done | bytes 524320 | tf_op jit(solution)/shard_map/ppermute | solution.py:22
  55.7 9.8 %collective-permute-done.3 = bf16[128,2048]{1,0:T(8,128)(2,1)S(1)} collective-permute-done((bf16[128,2048]{1,0:T(8,128)(2,1)S(1)}, bf16[128,2048]{1,0:T(8,128)(2,1)S(1)}, u32[]{:S(2)}, u32[]{:S(2)}) %collective-permute-start.3) | collective-permute-done | bytes 524320 | tf_op jit(solution)/shard_map/ppermute | solution.py:22
  65.6 1.5 broadcast_in_dim.19
  67.2 9.5 %all-to-all-start = ((bf16[16,512,128]{1,2,0:T(8,128)(2,1)}), bf16[16,512,128]{1,2,0:T(8,128)(2,1)}, u32[]{:S(2)}, u32[]{:S(2)}) async-start(bf16[16,512,128]{1,2,0:T(8,128)(2,1)} %broadcast_in_dim.19), calls=%async_computation | async-start | bytes 4194304 | tf_op jit(solution)/shard_map/all_to_all | solution.py:34
  80.0 5.5 %collective-permute-done.5 = bf16[128,2048]{1,0:T(8,128)(2,1)S(1)} collective-permute-done((bf16[128,2048]{1,0:T(8,128)(2,1)}, bf16[128,2048]{1,0:T(8,128)(2,1)S(1)}, u32[]{:S(2)}, u32[]{:S(2)}) %collective-permute-start.5) | collective-permute-done | bytes 524320 | tf_op jit(solution)/shard_map/ppermute | solution.py:22
  87.1 1.9 constant_dynamic-update-slice_fusion.10
  89.9 5.3 %collective-permute-done.6 = bf16[128,2048]{1,0:T(8,128)(2,1)S(1)} collective-permute-done((bf16[128,2048]{1,0:T(8,128)(2,1)S(1)}, bf16[128,2048]{1,0:T(8,128)(2,1)S(1)}, u32[]{:S(2)}, u32[]{:S(2)}) %collective-permute-start.6) | collective-permute-done | bytes 524320 | tf_op jit(solution)/shard_map/ppermute | solution.py:22
  96.1 98.2 %all-gather.3.cloned.1.call-done = bf16[2048,1536]{1,0:T(8,128)(2,1)} async-done(((bf16[128,1536]{1,0:T(8,128)(2,1)}), bf16[2048,1536]{1,0:T(8,128)(2,1)}) %all-gather.3.cloned.1.call-update) | async-done | bytes 6291472 | tf_op jit(solution)/shard_map/all_gather | solution.py:58
  194.3 3.9 convolution_bitcast_fusion.2
  198.7 3.4 convolution_bitcast_fusion.3
  202.2 2.3 subtract_convert_fusion
  205.4 1.1 fusion.43
  206.5 5.5 %fusion.34 = bf16[1024,512]{1,0:T(8,128)(2,1)} fusion(bf16[1024,2048]{1,0:T(8,128)(2,1)} %constant_dynamic-update-slice_fusion.8, bf16[2048,1536]{1,0:T(8,128)(2,1)S(1)} %copy-done.7), kind=kOutput, calls=%fused_computation.46 | convolution fusion | flops 2148007936 | bytes 7340032 | tf_op jit(solution)/shard_map/dot_general | solution.py:72
  212.0 25.3 %while.15 = (s32[]{:T(128)}, f32[1,256,512]{2,1,0:T(8,128)S(1)}, f32[8,128,1,512]{3,1,2,0:T(8,128)}, f32[1]{0:T(128)}, bf16[8,128,1,256]{3,2,1,0:T(2,128)(2,1)S(...) while((s32[]{:T(128)}, f32[1,256,512]{2,1,0:T(8,128)S(1)}, ...), condition=%wide.region_2.3_spmd.clone.clone.clone, body=%wide.region_1.2_spmd.clone.clone.clone.sunk | while | flops 67797504 | bytes 2232440 | solution.py:132
  212.1 1.8 fusion.100
  214.0 1.2 fusion.99
  215.2 1.7 fusion.100
  217.2 1.2 fusion.99
  218.4 1.8 fusion.100
  220.4 1.2 fusion.99
  221.6 1.7 fusion.100
  223.5 1.2 fusion.99
  224.7 1.7 fusion.100
  226.7 1.2 fusion.99
  227.9 1.7 fusion.100
  229.8 1.2 fusion.99
  231.1 1.8 fusion.100
  233.0 1.2 fusion.99
  234.2 1.7 fusion.100
  236.2 1.2 fusion.99
  237.4 2.8 fusion.74
  240.6 6.5 %fusion.27 = bf16[1024,512]{1,0:T(8,128)(2,1)} fusion(f32[8,128,1,512]{3,1,0,2:T(8,128)S(1)} %get-tuple-element.183, bf16[1024,2048]{1,0:T(8,128)(2,1)} %constant_dynamic-update-slice_fusion.8, bf16[2048,1536]{1,0:T(8,128)(2,1)} %all-gather.3.cloned.1.call-done, f32[1024]{0:T(1024)S(1)} %rsqrt_bitcast_fusion, f32[1024]{0:T(1024)S(1)} %get-tuple-element.178), kind=kOutput, calls=%fused_computation.36 | convolution fusion | flops 2151677952 | bytes 9445376 | tf_op jit(solution)/shard_map/dot_general | solution.py:72
  247.2 6.2 %convolution_convert_fusion.1 = bf16[1024,2048]{1,0:T(8,128)(2,1)} fusion(bf16[1024,512]{1,0:T(8,128)(2,1)} %fusion.27, bf16[512,2048]{0,1:T(8,128)(2,1)} %bitcast.26), kind=kOutput, calls=%fused_computation.27 | convolution fusion | flops 2149580800 | bytes 7340032 | tf_op jit(solution)/shard_map/dot_general | solution.py:78
  253.4 8.8 %all-to-all-start.1 = ((bf16[8,128,2048]{2,1,0:T(8,128)(2,1)}), bf16[8,128,2048]{2,1,0:T(8,128)(2,1)}, u32[]{:S(2)}, u32[]{:S(2)}) async-start(bf16[8,128,2048]{2,1,0:T(8,128)(2,1)} %bitcast.129), calls=%async_computation.1 | async-start | bytes 8388608 | tf_op jit(solution)/shard_map/all_to_all | solution.py:48
  263.1 47.9 %all-to-all-done.1 = bf16[8,128,2048]{2,1,0:T(8,128)(2,1)} async-done(((bf16[8,128,2048]{2,1,0:T(8,128)(2,1)}), bf16[8,128,2048]{2,1,0:T(8,128)(2,1)}, u32[]{:S(2)}, u32[]{:S(2)}) %all-to-all-start.1) | async-done | bytes 4194336 | tf_op jit(solution)/shard_map/all_to_all | solution.py:48
  311.0 1.4 broadcast_in_dim.20
  312.3 7.8 %all-to-all-start.2 = ((bf16[16,384,128]{1,2,0:T(8,128)(2,1)}), bf16[16,384,128]{1,2,0:T(8,128)(2,1)S(1)}, u32[]{:S(2)}, u32[]{:S(2)}) async-start(bf16[16,384,128]{1,2,0:T(8,128)(2,1)} %broadcast_in_dim.20), calls=%async_computation.2 | async-start | bytes 3145728 | tf_op jit(solution)/shard_map/all_to_all | solution.py:34
  320.1 3.0 convert_reduce_fusion.1
  323.7 2.5 broadcast.249
  326.2 1.1 constant_dynamic-update-slice_fusion.7
  327.3 1.5 collective-permute-start.7
  328.8 6.1 %collective-permute-done.7 = bf16[128,2048]{1,0:T(8,128)(2,1)S(1)} collective-permute-done((bf16[128,2048]{1,0:T(8,128)(2,1)S(1)}, bf16[128,2048]{1,0:T(8,128)(2,1)S(1)}, u32[]{:S(2)}, u32[]{:S(2)}) %collective-permute-start.7) | collective-permute-done | bytes 524320 | tf_op jit(solution)/shard_map/ppermute | solution.py:22
  334.9 2.5 collective-permute-start.8
  337.4 6.1 %collective-permute-done.8 = bf16[128,2048]{1,0:T(8,128)(2,1)S(1)} collective-permute-done((bf16[128,2048]{1,0:T(8,128)(2,1)S(1)}, bf16[128,2048]{1,0:T(8,128)(2,1)S(1)}, u32[]{:S(2)}, u32[]{:S(2)}) %collective-permute-start.8) | collective-permute-done | bytes 524320 | tf_op jit(solution)/shard_map/ppermute | solution.py:22
  343.5 2.5 collective-permute-start.9
  346.0 6.1 %collective-permute-done.9 = bf16[128,2048]{1,0:T(8,128)(2,1)S(1)} collective-permute-done((bf16[128,2048]{1,0:T(8,128)(2,1)S(1)}, bf16[128,2048]{1,0:T(8,128)(2,1)S(1)}, u32[]{:S(2)}, u32[]{:S(2)}) %collective-permute-start.9) | collective-permute-done | bytes 524320 | tf_op jit(solution)/shard_map/ppermute | solution.py:22
  352.1 2.5 collective-permute-start.10
  354.6 6.1 %collective-permute-done.10 = bf16[128,2048]{1,0:T(8,128)(2,1)S(1)} collective-permute-done((bf16[128,2048]{1,0:T(8,128)(2,1)S(1)}, bf16[128,2048]{1,0:T(8,128)(2,1)S(1)}, u32[]{:S(2)}, u32[]{:S(2)}) %collective-permute-start.10) | collective-permute-done | bytes 524320 | tf_op jit(solution)/shard_map/ppermute | solution.py:22
  360.7 2.5 collective-permute-start.11
  363.2 6.1 %collective-permute-done.11 = bf16[128,2048]{1,0:T(8,128)(2,1)S(1)} collective-permute-done((bf16[128,2048]{1,0:T(8,128)(2,1)S(1)}, bf16[128,2048]{1,0:T(8,128)(2,1)S(1)}, u32[]{:S(2)}, u32[]{:S(2)}) %collective-permute-start.11) | collective-permute-done | bytes 524320 | tf_op jit(solution)/shard_map/ppermute | solution.py:22
  369.4 2.5 collective-permute-start.12
  374.4 4.7 collective-permute-done.12
  379.0 1.4 collective-permute-start.13
  382.9 5.9 %collective-permute-done.13 = bf16[128,2048]{1,0:T(8,128)(2,1)S(1)} collective-permute-done((bf16[128,2048]{1,0:T(8,128)(2,1)S(1)}, bf16[128,2048]{1,0:T(8,128)(2,1)S(1)}, u32[]{:S(2)}, u32[]{:S(2)}) %collective-permute-start.13) | collective-permute-done | bytes 524320 | tf_op jit(solution)/shard_map/ppermute | solution.py:22
  389.7 6.2 %fusion.28 = f32[1024,384]{1,0:T(8,128)} fusion(bf16[1024,2048]{1,0:T(8,128)(2,1)} %constant_dynamic-update-slice_fusion, bf16[2048,768]{1,0:T(8,128)(2,1)} %all-gather.5.cloned.1.call-done), kind=kOutput, calls=%fused_computation.38 | convolution fusion | flops 1610612736 | bytes 7340032 | tf_op jit(solution)/shard_map/dot_general | solution.py:182
  396.0 9.6 %convolution_convert_fusion = bf16[1024,2048]{1,0:T(8,128)(2,1)} fusion(bf16[384,2048]{0,1:T(8,128)(2,1)S(1)} %bitcast.137, f32[1024,384]{1,0:T(8,128)} %fusion.28, bf16[1024,2048]{1,0:T(8,128)(2,1)} %constant_dynamic-update-slice_fusion, bf16[2048,768]{1,0:T(8,128)(2,1)} %all-gather.5.cloned.1.call-done), kind=kOutput, calls=%fused_computation.26 | convolution fusion | flops 3225681920 | bytes 13107200 | tf_op jit(solution)/shard_map/dot_general | solution.py:78
  405.6 60.7 %all_to_all.20 = bf16[8,128,2048]{2,1,0:T(8,128)(2,1)S(1)} all-to-all(bf16[8,128,2048]{2,1,0:T(8,128)(2,1)} %bitcast.130), channel_id=1, replica_groups=mesh['grp'=2,'fs'=16,'tp'=8] {'tp'}, dimensions={0} | all-to-all | bytes 8388608 | tf_op jit(solution)/shard_map/all_to_all | solution.py:48
  467.2 1.2 add_convert_fusion
  (81 shorter events, 20.3 us)
Async XLA Ops:
  6.5 6.7 %copy-start = (bf16[128,2048]{1,0:T(8,128)(2,1)S(1)}, bf16[128,2048]{1,0:T(8,128)(2,1)}, u32[]{:S(2)}) copy-start(bf16[128,2048]{1,0:T(8,128)(2,1)} %param.12) | copy-start | bytes 1572868
  6.5 58.9 %copy-start.3 = (bf16[512,128]{1,0:T(8,128)(2,1)S(1)}, bf16[512,128]{1,0:T(8,128)(2,1)}, u32[]{:S(2)}) copy-start(bf16[512,128]{1,0:T(8,128)(2,1)} %param.18) | copy-start | bytes 393220
  6.6 187.8 %all-gather.3.cloned.1.call-start = ((), (), s32[]{:S(2)}) async-start(), calls=%async_computation.4 | async-start | bytes 6684672 | tf_op jit(solution)/shard_map/all_gather | solution.py:58
  14.2 21.8 %collective-permute-start = (bf16[128,2048]{1,0:T(8,128)(2,1)S(1)}, bf16[128,2048]{1,0:T(8,128)(2,1)S(1)}, u32[]{:S(2)}, u32[]{:S(2)}) collective-permute-start(bf16[128,2048]{1,0:T(8,128)(2,1)S(1)} %get-tuple-element.167), channel_id=1, source_target_pairs={{0,1},{1,2},{2,3},{3,4},{4,5},{5,6},{6,7},{7,0},{8,9},{9,10},{10,1... | collective-permute-start | bytes 1572872 | tf_op jit(solution)/shard_map/ppermute | solution.py:22
  36.0 9.8 %collective-permute-start.1 = (bf16[128,2048]{1,0:T(8,128)(2,1)S(1)}, bf16[128,2048]{1,0:T(8,128)(2,1)S(1)}, u32[]{:S(2)}, u32[]{:S(2)}) collective-permute-start(bf16[128,2048]{1,0:T(8,128)(2,1)S(1)} %collective-permute-done), channel_id=1, source_target_pairs={{0,1},{1,2},{2,3},{3,4},{4,5},{5,6},{6,7},{7,0},{8,9},{9,10},{10,1... | collective-permute-start | bytes 1572872 | tf_op jit(solution)/shard_map/ppermute | solution.py:22
  45.9 9.8 %collective-permute-start.2 = (bf16[128,2048]{1,0:T(8,128)(2,1)S(1)}, bf16[128,2048]{1,0:T(8,128)(2,1)S(1)}, u32[]{:S(2)}, u32[]{:S(2)}) collective-permute-start(bf16[128,2048]{1,0:T(8,128)(2,1)S(1)} %collective-permute-done.1), channel_id=1, source_target_pairs={{0,1},{1,2},{2,3},{3,4},{4,5},{5,6},{6,7},{7,0},{8,9},{9,10},{10,1... | collective-permute-start | bytes 1572872 | tf_op jit(solution)/shard_map/ppermute | solution.py:22
  55.7 9.8 %collective-permute-start.3 = (bf16[128,2048]{1,0:T(8,128)(2,1)S(1)}, bf16[128,2048]{1,0:T(8,128)(2,1)S(1)}, u32[]{:S(2)}, u32[]{:S(2)}) collective-permute-start(bf16[128,2048]{1,0:T(8,128)(2,1)S(1)} %collective-permute-done.2), channel_id=1, source_target_pairs={{0,1},{1,2},{2,3},{3,4},{4,5},{5,6},{6,7},{7,0},{8,9},{9,10},{10,1... | collective-permute-start | bytes 1572872 | tf_op jit(solution)/shard_map/ppermute | solution.py:22
  65.5 11.6 %collective-permute-start.4 = (bf16[128,2048]{1,0:T(8,128)(2,1)S(1)}, bf16[128,2048]{1,0:T(8,128)(2,1)}, u32[]{:S(2)}, u32[]{:S(2)}) collective-permute-start(bf16[128,2048]{1,0:T(8,128)(2,1)S(1)} %collective-permute-done.3), channel_id=1, source_target_pairs={{0,1},{1,2},{2,3},{3,4},{4,5},{5,6},{6,7},{7,0},{8,9},{9,10},{10,1... | collective-permute-start | bytes 1572872 | tf_op jit(solution)/shard_map/ppermute | solution.py:22
  67.2 180.0 %all-to-all-start = ((bf16[16,512,128]{1,2,0:T(8,128)(2,1)}), bf16[16,512,128]{1,2,0:T(8,128)(2,1)}, u32[]{:S(2)}, u32[]{:S(2)}) async-start(bf16[16,512,128]{1,2,0:T(8,128)(2,1)} %broadcast_in_dim.19), calls=%async_computation | async-start | bytes 4194304 | tf_op jit(solution)/shard_map/all_to_all | solution.py:34
  77.1 8.3 %collective-permute-start.5 = (bf16[128,2048]{1,0:T(8,128)(2,1)}, bf16[128,2048]{1,0:T(8,128)(2,1)S(1)}, u32[]{:S(2)}, u32[]{:S(2)}) collective-permute-start(bf16[128,2048]{1,0:T(8,128)(2,1)} %collective-permute-done.4), channel_id=1, source_target_pairs={{0,1},{1,2},{2,3},{3,4},{4,5},{5,6},{6,7},{7,0},{8,9},{9,10},{10,1... | collective-permute-start | bytes 1572872 | tf_op jit(solution)/shard_map/ppermute | solution.py:22
  85.4 9.8 %collective-permute-start.6 = (bf16[128,2048]{1,0:T(8,128)(2,1)S(1)}, bf16[128,2048]{1,0:T(8,128)(2,1)S(1)}, u32[]{:S(2)}, u32[]{:S(2)}) collective-permute-start(bf16[128,2048]{1,0:T(8,128)(2,1)S(1)} %collective-permute-done.5), channel_id=1, source_target_pairs={{0,1},{1,2},{2,3},{3,4},{4,5},{5,6},{6,7},{7,0},{8,9},{9,10},{10,1... | collective-permute-start | bytes 1572872 | tf_op jit(solution)/shard_map/ppermute | solution.py:22
  194.3 4.4 copy-start.7
  204.4 1.0 copy-start.2
  204.4 7.6 %copy-start.1 = (f32[1024,1,128]{2,0,1:T(8,128)}, f32[1024,1,128]{2,0,1:T(8,128)S(1)}, u32[]{:S(2)}) copy-start(f32[1024,1,128]{2,0,1:T(8,128)S(1)} %get-tuple-element.181) | copy-start | bytes 1572868
  253.4 8.8 %copy-start.5 = (bf16[128,384]{1,0:T(8,128)(2,1)S(1)}, bf16[128,384]{1,0:T(8,128)(2,1)}, u32[]{:S(2)}) copy-start(bf16[128,384]{1,0:T(8,128)(2,1)} %param.20) | copy-start | bytes 294916
  253.4 8.8 %copy-start.6 = (bf16[128,384]{1,0:T(8,128)(2,1)S(1)}, bf16[128,384]{1,0:T(8,128)(2,1)}, u32[]{:S(2)}) copy-start(bf16[128,384]{1,0:T(8,128)(2,1)} %param.19) | copy-start | bytes 294916
  253.4 9.5 %copy-start.4 = (bf16[384,128]{1,0:T(8,128)(2,1)S(1)}, bf16[384,128]{1,0:T(8,128)(2,1)}, u32[]{:S(2)}) copy-start(bf16[384,128]{1,0:T(8,128)(2,1)} %param.21) | copy-start | bytes 294916
  253.4 57.5 %all-to-all-start.1 = ((bf16[8,128,2048]{2,1,0:T(8,128)(2,1)}), bf16[8,128,2048]{2,1,0:T(8,128)(2,1)}, u32[]{:S(2)}, u32[]{:S(2)}) async-start(bf16[8,128,2048]{2,1,0:T(8,128)(2,1)} %bitcast.129), calls=%async_computation.1 | async-start | bytes 8388608 | tf_op jit(solution)/shard_map/all_to_all | solution.py:48
  262.2 127.6 %all-gather.5.cloned.1.call-start = ((), (), s32[]{:S(2)}) async-start(), calls=%async_computation.5 | async-start | bytes 3342336 | tf_op jit(solution)/shard_map/all_gather | solution.py:58
  312.3 83.7 %all-to-all-start.2 = ((bf16[16,384,128]{1,2,0:T(8,128)(2,1)}), bf16[16,384,128]{1,2,0:T(8,128)(2,1)S(1)}, u32[]{:S(2)}, u32[]{:S(2)}) async-start(bf16[16,384,128]{1,2,0:T(8,128)(2,1)} %broadcast_in_dim.20), calls=%async_computation.2 | async-start | bytes 3145728 | tf_op jit(solution)/shard_map/all_to_all | solution.py:34
  327.3 7.6 %collective-permute-start.7 = (bf16[128,2048]{1,0:T(8,128)(2,1)S(1)}, bf16[128,2048]{1,0:T(8,128)(2,1)S(1)}, u32[]{:S(2)}, u32[]{:S(2)}) collective-permute-start(bf16[128,2048]{1,0:T(8,128)(2,1)S(1)} %get-tuple-element.165), channel_id=1, source_target_pairs={{0,1},{1,2},{2,3},{3,4},{4,5},{5,6},{6,7},{7,0},{8,9},{9,10},{10,1... | collective-permute-start | bytes 1572872 | tf_op jit(solution)/shard_map/ppermute | solution.py:22
  334.9 8.6 %collective-permute-start.8 = (bf16[128,2048]{1,0:T(8,128)(2,1)S(1)}, bf16[128,2048]{1,0:T(8,128)(2,1)S(1)}, u32[]{:S(2)}, u32[]{:S(2)}) collective-permute-start(bf16[128,2048]{1,0:T(8,128)(2,1)S(1)} %collective-permute-done.7), channel_id=1, source_target_pairs={{0,1},{1,2},{2,3},{3,4},{4,5},{5,6},{6,7},{7,0},{8,9},{9,10},{10,1... | collective-permute-start | bytes 1572872 | tf_op jit(solution)/shard_map/ppermute | solution.py:22
  343.5 8.6 %collective-permute-start.9 = (bf16[128,2048]{1,0:T(8,128)(2,1)S(1)}, bf16[128,2048]{1,0:T(8,128)(2,1)S(1)}, u32[]{:S(2)}, u32[]{:S(2)}) collective-permute-start(bf16[128,2048]{1,0:T(8,128)(2,1)S(1)} %collective-permute-done.8), channel_id=1, source_target_pairs={{0,1},{1,2},{2,3},{3,4},{4,5},{5,6},{6,7},{7,0},{8,9},{9,10},{10,1... | collective-permute-start | bytes 1572872 | tf_op jit(solution)/shard_map/ppermute | solution.py:22
  352.1 8.6 %collective-permute-start.10 = (bf16[128,2048]{1,0:T(8,128)(2,1)S(1)}, bf16[128,2048]{1,0:T(8,128)(2,1)S(1)}, u32[]{:S(2)}, u32[]{:S(2)}) collective-permute-start(bf16[128,2048]{1,0:T(8,128)(2,1)S(1)} %collective-permute-done.9), channel_id=1, source_target_pairs={{0,1},{1,2},{2,3},{3,4},{4,5},{5,6},{6,7},{7,0},{8,9},{9,10},{10,1... | collective-permute-start | bytes 1572872 | tf_op jit(solution)/shard_map/ppermute | solution.py:22
  360.7 8.6 %collective-permute-start.11 = (bf16[128,2048]{1,0:T(8,128)(2,1)S(1)}, bf16[128,2048]{1,0:T(8,128)(2,1)S(1)}, u32[]{:S(2)}, u32[]{:S(2)}) collective-permute-start(bf16[128,2048]{1,0:T(8,128)(2,1)S(1)} %collective-permute-done.10), channel_id=1, source_target_pairs={{0,1},{1,2},{2,3},{3,4},{4,5},{5,6},{6,7},{7,0},{8,9},{9,10},{10,1... | collective-permute-start | bytes 1572872 | tf_op jit(solution)/shard_map/ppermute | solution.py:22
  369.4 9.7 %collective-permute-start.12 = (bf16[128,2048]{1,0:T(8,128)(2,1)S(1)}, bf16[128,2048]{1,0:T(8,128)(2,1)S(1)}, u32[]{:S(2)}, u32[]{:S(2)}) collective-permute-start(bf16[128,2048]{1,0:T(8,128)(2,1)S(1)} %collective-permute-done.11), channel_id=1, source_target_pairs={{0,1},{1,2},{2,3},{3,4},{4,5},{5,6},{6,7},{7,0},{8,9},{9,10},{10,1... | collective-permute-start | bytes 1572872 | tf_op jit(solution)/shard_map/ppermute | solution.py:22
  379.0 9.8 %collective-permute-start.13 = (bf16[128,2048]{1,0:T(8,128)(2,1)S(1)}, bf16[128,2048]{1,0:T(8,128)(2,1)S(1)}, u32[]{:S(2)}, u32[]{:S(2)}) collective-permute-start(bf16[128,2048]{1,0:T(8,128)(2,1)S(1)} %collective-permute-done.12), channel_id=1, source_target_pairs={{0,1},{1,2},{2,3},{3,4},{4,5},{5,6},{6,7},{7,0},{8,9},{9,10},{10,1... | collective-permute-start | bytes 1572872 | tf_op jit(solution)/shard_map/ppermute | solution.py:22
Sparse Core Ops, SparseCore 0:
  9.2 185.1 all-gather.2
  264.8 73.3 all-gather.4
